TPU v7x, 32 devices: a whole 2x2x4 slice. The times are simulated.
32 devices in a mesh: kv: 8 (over z, x), tp: 4 (over y, core).
Axes of the slice: x: 2, y: 2, z: 4, core: 2. Of those that a mesh axis runs over, the one named last changes fastest.
Arguments:
- tokens: bfloat16 [4096, 2048], P('kv'), may hold values from -64 to 64
- query_weight: bfloat16 [2048, 2048], P(None, 'tp'), may hold values from -0.1875 to 0.1875
- chosen_key_weight: bfloat16 [2048, 512], P(None, 'tp'), may hold values from -0.125 to 0.125
- chosen_value_weight: bfloat16 [2048, 512], P(None, 'tp'), may hold values from -0.125 to 0.125
- summary_key_weight: bfloat16 [2048, 512], P(None, 'tp'), may hold values from -0.125 to 0.125
- summary_value_weight: bfloat16 [2048, 512], P(None, 'tp'), may hold values from -0.125 to 0.125
- squeeze_key_in: bfloat16 [2048, 128], replicated, may hold values from -0.125 to 0.125
- squeeze_key_out: bfloat16 [128, 64], replicated, may hold values from -1 to 1
- squeeze_value_in: bfloat16 [2048, 128], replicated, may hold values from -0.125 to 0.125
- squeeze_value_out: bfloat16 [128, 64], replicated, may hold values from -2 to 2
- gate_weight: bfloat16 [2, 2048, 32], P(None, None, 'tp'), may hold values from -0.125 to 0.125
- output_weight: bfloat16 [2048, 2048], P('tp'), may hold values from -1 to 1
- chosen_blocks: int32 [8, 128, 16], P('tp', 'kv'), may hold values from 0 to 127, as said below
Outputs:
- attended: bfloat16 [4096, 2048], P(('kv', 'tp'))
Inputs may be any that keep to these rules, and one draw needn't show every extreme that they name: `chosen_blocks`: each row lists 16 different blocks. The row of query block b lists b, lists b - 1 where b > 0, and lists block 0. Take the blocks at or below their query block that the rows of the query blocks of one index of kv list for one key head: at most 4 different ones lie among the positions of any other single index of kv, and exactly 4 among the positions of the first index, for every index after the first.
All inputs are finite; a program needn't handle non-finite values.
Results may differ from a plain program's by a relative error of at most 0.03.
Values may be sent and summed in bfloat16 or wider, within the bound.
A program may use at most 128 MiB of HBM per device.

v0:
```python
import jax
import jax.numpy as jnp
from jax import lax
from jax.sharding import PartitionSpec as P

HD = 64
CMP_LEN = 32
CMP_STRIDE = 16
BLK = 32
ROTARY_BASE = 10000.0
NEGATIVE_FILL = -1e30


def from_behind(block, axis, distance):
    devices = range(lax.axis_size(axis))
    route = [(i - distance, i) for i in devices if i - distance in devices]
    return lax.ppermute(block, axis, route)


def rotate(values, positions):
    halfway = values.shape[-1] // 2
    inverse = ROTARY_BASE ** (-jnp.arange(halfway, dtype=jnp.float32) / halfway)
    angles = positions.astype(jnp.float32)[:, None] * inverse[None, :]
    cosine_rows = jnp.cos(angles)[:, None, :]
    sine_rows = jnp.sin(angles)[:, None, :]
    former = values[..., :halfway]
    latter = values[..., halfway:]
    return jnp.concatenate(
        [former * cosine_rows - latter * sine_rows, latter * cosine_rows + former * sine_rows], -1
    )


def squeeze_windows(windows, weight_in, weight_out):
    total_windows = windows.shape[0]
    groups = windows.shape[2]
    head_width = windows.shape[3]
    flattened = windows.transpose(0, 2, 1, 3).reshape(total_windows * groups, CMP_LEN * head_width)
    hidden = jax.nn.gelu(jnp.dot(flattened, weight_in, preferred_element_type=jnp.float32)).astype(
        jnp.bfloat16
    )
    return jnp.dot(hidden, weight_out, preferred_element_type=jnp.float32).reshape(
        total_windows, groups, head_width
    )


def online_step(running, scores, visible, values):
    largest, summed, weighted = running
    updated = jnp.maximum(largest, jnp.max(jnp.where(visible, scores, NEGATIVE_FILL), -1))
    weights = jnp.where(visible, jnp.exp(scores - updated[..., None]), 0.0)
    shrink = jnp.exp(largest - updated)
    summed = summed * shrink + jnp.sum(weights, -1)
    weighted = weighted * shrink[..., None] + jnp.einsum(
        "grqk,kgd->grqd", weights.astype(jnp.bfloat16), values, preferred_element_type=jnp.float32
    )
    return (updated, summed, weighted)


def on_device(
    tokens,
    query_weight,
    chosen_key_weight,
    chosen_value_weight,
    summary_key_weight,
    summary_value_weight,
    squeeze_key_in,
    squeeze_key_out,
    squeeze_value_in,
    squeeze_value_out,
    gate_weight,
    output_weight,
    chosen_blocks,
):
    tok_rows = tokens.shape[0]
    heads_here = query_weight.shape[1] // HD
    groups_here = chosen_key_weight.shape[1] // HD
    per_group = heads_here // groups_here
    kv_rank = lax.axis_index("kv")
    offset = kv_rank * tok_rows
    positions = offset + jnp.arange(tok_rows, dtype=jnp.int32)
    queries = rotate(
        jnp.dot(tokens, query_weight, preferred_element_type=jnp.float32).reshape(
            tok_rows, heads_here, HD
        ),
        positions,
    )
    queries = queries.astype(jnp.bfloat16).reshape(tok_rows, groups_here, per_group, HD)
    chosen_keys = rotate(
        jnp.dot(tokens, chosen_key_weight, preferred_element_type=jnp.float32).reshape(
            tok_rows, groups_here, HD
        ),
        positions,
    ).astype(jnp.bfloat16)
    chosen_values = (
        jnp.dot(tokens, chosen_value_weight, preferred_element_type=jnp.float32)
        .astype(jnp.bfloat16)
        .reshape(tok_rows, groups_here, HD)
    )
    chosen_pairs = jnp.concatenate([chosen_keys, chosen_values], -1)
    raw_keys = (
        jnp.dot(tokens, summary_key_weight, preferred_element_type=jnp.float32)
        .astype(jnp.bfloat16)
        .reshape(tok_rows, groups_here, HD)
    )
    raw_values = (
        jnp.dot(tokens, summary_value_weight, preferred_element_type=jnp.float32)
        .astype(jnp.bfloat16)
        .reshape(tok_rows, groups_here, HD)
    )
    raw_pairs = jnp.concatenate([raw_keys, raw_values], -1)
    following = from_behind(raw_pairs[:CMP_STRIDE], "kv", -1)
    extended = jnp.concatenate([raw_pairs, following], 0)
    summary_count = tok_rows // CMP_STRIDE
    segments = extended.reshape(summary_count + 1, CMP_STRIDE, groups_here, 2 * HD)
    windows = jnp.concatenate([segments[:-1], segments[1:]], 1)
    summary_ends = (
        (kv_rank * summary_count + jnp.arange(summary_count, dtype=jnp.int32)) * CMP_STRIDE
        + CMP_LEN
        - 1
    )
    summary_keys = rotate(
        squeeze_windows(windows[..., :HD], squeeze_key_in, squeeze_key_out), summary_ends
    ).astype(jnp.bfloat16)
    summary_values = squeeze_windows(windows[..., HD:], squeeze_value_in, squeeze_value_out).astype(
        jnp.bfloat16
    )
    summaries = jnp.concatenate([summary_keys, summary_values], -1)
    scaling = HD ** (-0.5)
    starting = (
        jnp.full((groups_here, per_group, tok_rows), NEGATIVE_FILL, jnp.float32),
        jnp.zeros((groups_here, per_group, tok_rows), jnp.float32),
        jnp.zeros((groups_here, per_group, tok_rows, HD), jnp.float32),
    )
    portion = lax.all_gather(summaries, "kv", axis=0, tiled=True)
    length = portion.shape[0]
    ends = jnp.arange(length, dtype=jnp.int32) * CMP_STRIDE + CMP_LEN - 1
    scores = (
        jnp.einsum("qgrd,kgd->grqk", queries, portion[..., :HD], preferred_element_type=jnp.float32)
        * scaling
    )
    visible = (ends[None, :] <= positions[:, None])[None, None]
    folded = online_step(starting, scores, visible, portion[..., HD:])
    compressed = folded[2] / jnp.maximum(folded[1], 1.0)[..., None]
    block_count = tok_rows // BLK

    def span_step(running, stretch, leading):
        length = stretch.shape[0]
        key_positions = leading + jnp.arange(length, dtype=jnp.int32)
        listed = jnp.any(
            chosen_blocks[:, :, :, None] == (key_positions // BLK)[None, None, None, :], axis=2
        )
        listed = jnp.broadcast_to(
            listed[:, :, None, :], (groups_here, block_count, BLK, length)
        ).reshape(groups_here, tok_rows, length)
        visible = (listed & (key_positions[None, None, :] <= positions[None, :, None]))[:, None]
        scores = (
            jnp.einsum(
                "qgrd,kgd->grqk", queries, stretch[..., :HD], preferred_element_type=jnp.float32
            )
            * scaling
        )
        return online_step(running, scores, visible, stretch[..., HD:])

    def maybe_step(running, stretch, leading):

        def step_taken(carried):
            return span_step(carried, stretch, leading)

        def step_skipped(carried):
            return carried

        return lax.cond(leading <= offset + tok_rows - 1, step_taken, step_skipped, running)

    portion = lax.all_gather(chosen_pairs, "kv", axis=0, tiled=True)
    length = portion.shape[0]
    stretch_rows = tok_rows * 4

    def visit_span(number, carried):
        stretch = lax.dynamic_slice_in_dim(portion, number * stretch_rows, stretch_rows, 0)
        return maybe_step(carried, stretch, number * stretch_rows)

    folded_chosen = lax.fori_loop(0, length // stretch_rows, visit_span, starting)
    selected = folded_chosen[2] / folded_chosen[1][..., None]
    first_gates = jax.nn.sigmoid(
        jnp.dot(tokens, gate_weight[0], preferred_element_type=jnp.float32)
    )
    second_gates = jax.nn.sigmoid(
        jnp.dot(tokens, gate_weight[1], preferred_element_type=jnp.float32)
    )
    first_gates = first_gates.reshape(tok_rows, groups_here, per_group).transpose(1, 2, 0)[
        ..., None
    ]
    second_gates = second_gates.reshape(tok_rows, groups_here, per_group).transpose(1, 2, 0)[
        ..., None
    ]
    blended = (
        (first_gates * compressed + second_gates * selected)
        .transpose(2, 0, 1, 3)
        .reshape(tok_rows, heads_here * HD)
        .astype(jnp.bfloat16)
    )
    attended = lax.psum_scatter(
        jnp.dot(blended, output_weight, preferred_element_type=jnp.float32).astype(jnp.bfloat16),
        "tp",
        scatter_dimension=0,
        tiled=True,
    )
    return attended


def solution(mesh):
    return jax.shard_map(
        on_device,
        mesh=mesh,
        in_specs=(
            P("kv", None),
            P(None, "tp"),
            P(None, "tp"),
            P(None, "tp"),
            P(None, "tp"),
            P(None, "tp"),
            P(),
            P(),
            P(),
            P(),
            P(None, None, "tp"),
            P("tp", None),
            P("tp", "kv", None),
        ),
        out_specs=P(("kv", "tp"), None),
        check_vma=False,
    )
```

profile of v0, /device:TPU:0, one launch (start us, length us, event | category | flops | bytes accessed | tf_op | source)
XLA Modules:
  0.0 240.7 jit_solution(17851520680205878891)
XLA Ops:
  6.6 2.7 %convolution_convert_fusion.1 = bf16[512,128]{0,1:T(8,128)(2,1)S(1)} fusion(bf16[512,2048]{1,0:T(8,128)(2,1)} %param.17, bf16[2048,128]{1,0:T(8,128)(2,1)} %param.20), kind=kOutput, calls=%fused_computation.44 | convolution fusion | flops 268500992 | bytes 2752512 | tf_op jit(solution)/shard_map/dot_general | solution.py:94
  9.2 2.5 %fusion.91 = f32[512,128]{0,1:T(8,128)S(1)} fusion(bf16[512,2048]{1,0:T(8,128)(2,1)} %param.17, bf16[2048,128]{1,0:T(8,128)(2,1)} %param.19), kind=kOutput, calls=%fused_computation.133 | convolution fusion | flops 268435456 | bytes 2883584 | tf_op jit(solution)/shard_map/dot_general | solution.py:88
  11.7 0.3 multiply_cosine_fusion
  12.1 0.7 pad_maximum_fusion.4
  12.9 2.4 %convolution_convert_fusion.2 = bf16[512,128]{0,1:T(8,128)(2,1)S(1)} fusion(bf16[512,2048]{1,0:T(8,128)(2,1)} %param.17, bf16[2048,128]{1,0:T(8,128)(2,1)S(1)} %copy-done.7), kind=kOutput, calls=%fused_computation.45 | convolution fusion | flops 268500992 | bytes 2752512 | tf_op jit(solution)/shard_map/dot_general | solution.py:105
  15.5 2.5 %convolution_convert_fusion.3 = bf16[512,128]{0,1:T(8,128)(2,1)S(1)} fusion(bf16[512,2048]{1,0:T(8,128)(2,1)} %param.17, bf16[2048,128]{1,0:T(8,128)(2,1)} %param.21), kind=kOutput, calls=%fused_computation.46 | convolution fusion | flops 268500992 | bytes 2752512 | tf_op jit(solution)/shard_map/dot_general | solution.py:100
  18.0 0.2 copy.52
  18.2 0.7 pad_maximum_fusion.6
  18.9 1.3 collective-permute-start
  20.2 3.5 %fusion.90 = f32[512,512]{0,1:T(8,128)S(1)} fusion(bf16[512,2048]{1,0:T(8,128)(2,1)} %param.17, bf16[2048,512]{1,0:T(8,128)(2,1)} %param.18), kind=kOutput, calls=%fused_computation.132 | convolution fusion | flops 1073741824 | bytes 5242880 | tf_op jit(solution)/shard_map/dot_general | solution.py:81
  24.0 0.7 multiply_cosine_fusion.1
  24.8 2.9 %fusion.34 = f32[512,8]{0,1:T(8,128)} fusion(bf16[512,2048]{1,0:T(8,128)(2,1)} %param.17, bf16[2,2048,8]{1,2,0:T(8,128)(2,1)} %param.27), kind=kOutput, calls=%fused_computation.51 | convolution fusion | flops 16789504 | bytes 2146304 | tf_op jit(solution)/shard_map/dot_general | solution.py:187
  27.7 2.3 fusion.37
  29.9 0.8 pad_maximum_fusion.1
  30.8 0.8 copy.51
  31.5 0.7 copy.50
  32.3 1.0 concatenate.38
  33.3 1.0 concatenate.37
  34.4 1.3 reshape.285
  35.7 0.6 reshape.278
  36.3 0.8 pad_maximum_fusion.2
  37.2 0.3 copy.54
  37.4 1.0 pad_maximum_fusion
  38.5 1.0 slice_bitcast_fusion.1
  39.6 0.5 reshape.283
  40.2 0.5 reshape.281
  40.6 1.4 fusion.64
  42.0 0.8 subtract_convert_fusion.2
  42.9 1.4 convolution_convert_fusion.4
  44.4 35.0 %all_gather.6 = bf16[256,2,128]{2,1,0:T(2,128)(2,1)S(1)} all-gather(bf16[32,2,128]{2,1,0:T(2,128)(2,1)S(1)} %pad_maximum_fusion.5), channel_id=1, replica_groups=mesh['kv'=8,'tp'=4] {'kv'}, dimensions={0}, use_global_device_ids=true | all-gather | bytes 147456 | tf_op jit(solution)/shard_map/all_gather | solution.py:133
  79.4 0.2 fusion.85
  79.8 0.7 copy.67
  80.5 1.9 fusion.21
  82.4 2.0 copy-done.2
  84.4 0.9 fusion.24
  85.3 0.6 exponential_multiply_fusion
  86.2 55.0 %while.20 = (s32[]{:T(128)}, f32[2,4,512]{2,1,0:T(4,128)S(1)}, f32[2,4,512]{2,1,0:T(4,128)S(1)}, f32[2,4,512,64]{2,3,1,0:T(8,128)S(1)}, s32[]{:T(128)}, /*index=...) while((s32[]{:T(128)}, f32[2,4,512]{2,1,0:T(4,128)S(1)}, ...), condition=%wide.region_8.9_spmd.clone, body=%wide.region_2.8_spmd.clone.sunk | while | flops 2245501440 | bytes 127838584 | solution.py:181
  86.2 54.9 %conditional.3 = ((f32[2,4,512]{2,1,0:T(4,128)S(1)}, f32[2,4,512]{2,1,0:T(4,128)S(1)}, f32[2,4,512,64]{2,3,1,0:T(8,128)S(1)})) conditional(s32[]{:T(128)} %convert_element_type.107, (f32[2,4,512]{2,1,0:T(4,128)S(1)}, f32[2,4,512]{2,1,0:T(4,128)S(1)}, f32[2,4,512,64]{2,3,1,0:T(8,128)S(1)}) %tuple.69, (s32[2,16,16]{2,1,0:T(8,128)S(1)}, s32[]{:T(128)}, ...), branch_computations={%region_3.3_spmd, %region_4.7_spmd} | conditional | flops 2245501440 | bytes 127836296 | solution.py:171
  86.3 0.7 broadcast_compare_fusion
  86.9 1.0 compare_reduce_fusion
  88.0 2.6 %bitcast_and_fusion = pred[2,512,2048]{2,1,0:T(8,128)(4,1)} fusion(pred[512,2048]{1,0:T(8,128)(4,1)S(1)} %broadcast_compare_fusion, pred[2,16,2048]{2,1,0:T(8,128)(4,1)S(1)} %compare_reduce_fusion), kind=kLoop, calls=%fused_computation.10 | loop fusion | flops 2097152 | bytes 3211264 | tf_op jit(solution)/shard_map/while/body/eval_jaxpr/cond/branch_1_fun/and | solution.py:154
  90.6 6.1 %copy.48 = pred[2,512,2048]{1,2,0:T(8,128)(4,1)} copy(pred[2,512,2048]{2,1,0:T(8,128)(4,1)} %bitcast_and_fusion) | data formatting | bytes 4194304 | tf_op jit(solution)/shard_map/while/body/eval_jaxpr/cond/branch_1_fun/and | solution.py:154
  96.6 15.2 %fusion.2 = (f32[2,4,512]{2,1,0:T(4,128)S(1)}, f32[2,2048,512,4]{2,1,3,0:T(8,128)}) fusion(pred[2,512,2048]{1,2,0:T(8,128)(4,1)} %copy.48, bf16[512,2,4,64]{0,3,2,1:T(8,128)(2,1)} %get-tuple-element.301, bf16[4096,2,128]{0,2,1:T(8,128)(2,1)} %get-tuple-element.300, s32[]{:T(128)S(6)} %select_n.35), kind=kOutput, calls=%fused_computation.3 | convolution fusion | flops 1098903552 | bytes 36716548 | tf_op jit(solution)/shard_map/while/body/eval_jaxpr/cond/branch_1_fun/qgrd,kgd->grqk/dot_general | solution.py:156
  111.9 14.3 %fusion.6 = f32[2,4,512]{2,1,0:T(4,128)S(1)} fusion(f32[2,2048,512,4]{2,1,3,0:T(8,128)} %get-tuple-element.369, f32[2,4,512]{2,1,0:T(4,128)S(1)} %max.12, pred[2,512,2048]{1,2,0:T(8,128)(4,1)S(1)} %copy-done.1), kind=kLoop, calls=%fused_computation.7 | loop fusion | flops 33550336 | bytes 35684352 | tf_op jit(solution)/shard_map/while/body/eval_jaxpr/cond/branch_1_fun/reduce_sum | solution.py:51
  126.2 14.9 %fusion.10 = f32[2,4,512,64]{2,3,1,0:T(8,128)S(1)} fusion(f32[2,2048,512,4]{2,1,3,0:T(8,128)} %get-tuple-element.369, f32[2,4,512]{2,1,0:T(4,128)S(1)} %max.12, pred[2,512,2048]{1,2,0:T(8,128)(4,1)} %copy.48, f32[2,4,512,64]{2,3,1,0:T(8,128)S(1)} %get-tuple-element.303, bf16[4096,2,128]{0,2,1:T(8,128)(2,1)} %get-tuple-element.300, s32[]{:T(128)S(6)} %select_n.35, ...), kind=kOutput, calls=%fused_computation.13 | convolution fusion | flops 1107820544 | bytes 38305800 | tf_op jit(solution)/shard_map/while/body/eval_jaxpr/cond/branch_1_fun/grqk,kgd->grqd/dot_general | solution.py:52
  141.3 3.3 %add_convert_fusion = bf16[2,4,512,64]{2,3,1,0:T(8,128)(2,1)S(1)} fusion(f32[2,4,512,64]{2,3,1,0:T(8,128)S(1)} %get-tuple-element.319, f32[2,256,512,4]{2,1,3,0:T(8,128)} %copy-done.2, f32[2,4,512]{2,1,0:T(4,128)} %copy-done.9, pred[512,256]{0,1:T(8,128)(4,1)S(1)} %copy-done.6, f32[2,4,512]{2,1,0:T(4,128)S(1)} %get-tuple-element.320, ...), kind=kOutput, calls=%fused_computation.56 | convolution fusion | flops 140247040 | bytes 6062080 | tf_op jit(solution)/shard_map/grqk,kgd->grqd/dot_general | solution.py:52
  144.5 2.6 %convolution_convert_fusion = bf16[512,2048]{1,0:T(8,128)(2,1)} fusion(bf16[512,512]{0,1:T(8,128)(2,1)S(1)} %bitcast.140, bf16[512,2048]{1,0:T(8,128)(2,1)S(1)} %copy-done), kind=kOutput, calls=%fused_computation.40 | convolution fusion | flops 1074790400 | bytes 4718592 | tf_op jit(solution)/shard_map/dot_general | solution.py:202
  147.2 86.7 %reduce-scatter.2.cloned.1.call-done = bf16[128,2048]{1,0:T(8,128)(2,1)} async-done(((bf16[512,2048]{1,0:T(8,128)(2,1)}), bf16[128,2048]{1,0:T(8,128)(2,1)}) %reduce-scatter.2.cloned.1.call-update) | async-done | bytes 524304 | tf_op jit(solution)/shard_map/reduce_scatter | solution.py:201
  (62 shorter events, 1.3 us)
Async XLA Ops:
  6.5 138.0 %copy-start = (bf16[512,2048]{1,0:T(8,128)(2,1)S(1)}, bf16[512,2048]{1,0:T(8,128)(2,1)}, u32[]{:S(2)}) copy-start(bf16[512,2048]{1,0:T(8,128)(2,1)} %param.28) | copy-start | bytes 6291460
  6.5 6.4 %copy-start.7 = (bf16[2048,128]{1,0:T(8,128)(2,1)S(1)}, bf16[2048,128]{1,0:T(8,128)(2,1)}, u32[]{:S(2)}) copy-start(bf16[2048,128]{1,0:T(8,128)(2,1)} %param.22) | copy-start | bytes 1572868
  6.5 79.4 %all-gather.2.cloned.1.call-start = ((), (), s32[]{:S(2)}) async-start(), calls=%async_computation.1 | async-start | bytes 2359296 | tf_op jit(solution)/shard_map/all_gather | solution.py:173
  12.8 221.0 %reduce-scatter.2.cloned.1.call-start = ((), (), s32[]{:S(2)}) async-start(), calls=%async_computation.2 | async-start | bytes 2621440 | tf_op jit(solution)/shard_map/reduce_scatter | solution.py:201
  18.9 17.5 %collective-permute-start = (bf16[16,2,128]{2,0,1:T(8,128)(2,1)}, bf16[16,2,128]{2,0,1:T(8,128)(2,1)}, u32[]{:S(2)}, u32[]{:S(2)}) collective-permute-start(bf16[16,2,128]{2,0,1:T(8,128)(2,1)} %pad_maximum_fusion.6), channel_id=1, source_target_pairs={{4,0},{8,4},{12,8},{16,12},{20,16},{24,20},{28,24},{5,1},{9,5},{13... | collective-permute-start | bytes 24584 | tf_op jit(solution)/shard_map/ppermute | solution.py:17
  23.9 8.4 %copy-start.3 = (bf16[512,8,32]{0,2,1:T(8,128)(2,1)}, bf16[512,8,32]{0,2,1:T(8,128)(2,1)S(1)}, u32[]{:S(2)}) copy-start(bf16[512,8,32]{0,2,1:T(8,128)(2,1)S(1)} %get-tuple-element.372) | copy-start | bytes 786436
  23.9 14.6 %copy-start.4 = (bf16[512,8,32]{0,2,1:T(8,128)(2,1)}, bf16[512,8,32]{0,2,1:T(8,128)(2,1)S(1)}, u32[]{:S(2)}) copy-start(bf16[512,8,32]{0,2,1:T(8,128)(2,1)S(1)} %get-tuple-element.373) | copy-start | bytes 786436
  24.0 58.4 %copy-start.5 = (pred[512,256]{0,1:T(8,128)(4,1)}, pred[512,256]{0,1:T(8,128)(4,1)S(1)}, u32[]{:S(2)}) copy-start(pred[512,256]{0,1:T(8,128)(4,1)S(1)} %broadcast_compare_fusion.1) | copy-start | bytes 393220
  37.2 4.9 %copy-start.11 = (f32[32,32]{1,0:T(8,128)S(1)}, f32[32,32]{1,0:T(8,128)}, u32[]{:S(2)}) copy-start(f32[32,32]{1,0:T(8,128)} %get-tuple-element.386) | copy-start | bytes 12292
  80.5 5.6 %copy-start.8 = (s32[2,16,16]{2,1,0:T(8,128)S(1)}, s32[2,16,16]{2,1,0:T(8,128)}, u32[]{:S(2)}) copy-start(s32[2,16,16]{2,1,0:T(8,128)} %param.29) | copy-start | bytes 6148
  82.4 2.1 copy-start.2
  82.4 3.8 %copy-start.9 = (f32[2,4,512]{2,1,0:T(4,128)}, f32[2,4,512]{2,1,0:T(4,128)S(1)}, u32[]{:S(2)}) copy-start(f32[2,4,512]{2,1,0:T(4,128)S(1)} %broadcast_maximum_fusion) | copy-start | bytes 49156
  86.1 55.1 %copy-start.6 = (pred[512,256]{0,1:T(8,128)(4,1)S(1)}, pred[512,256]{0,1:T(8,128)(4,1)}, u32[]{:S(2)}) copy-start(pred[512,256]{0,1:T(8,128)(4,1)} %copy-done.5) | copy-start | bytes 393220
  86.1 55.1 %copy-start.10 = (bf16[256,2,64]{0,2,1:T(8,128)(2,1)S(1)}, bf16[256,2,64]{0,2,1:T(8,128)(2,1)}, u32[]{:S(2)}) copy-start(bf16[256,2,64]{0,2,1:T(8,128)(2,1)} %copy.67) | copy-start | bytes 196612
  86.1 55.1 %copy-start.12 = (f32[512,2,4]{0,2,1:T(4,128)S(1)}, f32[512,2,4]{0,2,1:T(4,128)}, u32[]{:S(2)}) copy-start(f32[512,2,4]{0,2,1:T(4,128)} %reshape.285) | copy-start | bytes 49156
  86.1 55.1 %copy-start.13 = (f32[512,2,4]{0,2,1:T(4,128)S(1)}, f32[512,2,4]{0,2,1:T(4,128)}, u32[]{:S(2)}) copy-start(f32[512,2,4]{0,2,1:T(4,128)} %reshape.278) | copy-start | bytes 49156
  86.2 55.1 %copy-start.14 = (f32[2,4,512]{2,1,0:T(4,128)S(1)}, f32[2,4,512]{2,1,0:T(4,128)}, u32[]{:S(2)}) copy-start(f32[2,4,512]{2,1,0:T(4,128)} %get-tuple-element.382) | copy-start | bytes 49156
  86.2 55.1 %copy-start.15 = (f32[2,4,512]{2,1,0:T(4,128)S(1)}, f32[2,4,512]{2,1,0:T(4,128)}, u32[]{:S(2)}) copy-start(f32[2,4,512]{2,1,0:T(4,128)} %get-tuple-element.383) | copy-start | bytes 49156
  96.6 15.2 %copy-start.1 = (pred[2,512,2048]{1,2,0:T(8,128)(4,1)S(1)}, pred[2,512,2048]{1,2,0:T(8,128)(4,1)}, u32[]{:S(2)}) copy-start(pred[2,512,2048]{1,2,0:T(8,128)(4,1)} %copy.48) | copy-start | bytes 6291460 | tf_op jit(solution)/shard_map/while/body/eval_jaxpr/cond
Sparse Core Ops, SparseCore 0:
  13.0 54.0 all-gather.1
  147.3 86.5 reduce-scatter.1
where the time goes:
time: 242 us; the launch traced here: 241 us
  waiting for transfers between devices  86.8 us (36%)
  matrix products  59.3 us (25%)
  blocking collectives  35 us (14%)
  other arithmetic  26.6 us (11%)
  local copies, waits for them, and re-layouts  17.6 us (7%)
  between operations  13.8 us (6%)
    reduce_scatter x1, waiting for transfers between devices, on_device(): lax.psum_scatter(jnp.dot(blended, output_weight, preferred_element_type=j...  86.7 us
    all_gather x1, blocking collectives, on_device(): portion = lax.all_gather(summaries, 'kv', axis=0, tiled=True)  35 us
    dot_general x2, matrix products, online_step(): jnp.einsum('grqk,kgd->grqd', weights.astype(jnp.bfloat16), values, prefer...  18.1 us
    dot_general x1, matrix products, span_step(): jnp.einsum('qgrd,kgd->grqk', queries, stretch[..., :HD], preferred_elemen...  15.2 us
    reduce_sum x2, other arithmetic, online_step(): summed = summed * shrink + jnp.sum(weights, -1)  15.2 us
    and x1, local copies, waits for them, and re-layouts, span_step(): listed & (key_positions[None, None, :] <= positions[None, :, None])  6.06 us
  transfers between devices with their start and end apart: 3, of which 1 were waited for; matrix products, arithmetic and copies ran while one was open for 14% of the time, Pallas kernels for 0%

commit v1 on v0

--- a/solution.py
+++ b/solution.py
@@ -130,7 +130,12 @@
         jnp.zeros((groups_here, per_group, tok_rows), jnp.float32),
         jnp.zeros((groups_here, per_group, tok_rows, HD), jnp.float32),
     )
-    portion = lax.all_gather(summaries, "kv", axis=0, tiled=True)
+    ring = [summaries]
+    for hop in range(7):
+        ring.append(lax.ppermute(ring[-1], "kv", [(dev, (dev + 1) % 8) for dev in range(8)]))
+    portion = jnp.roll(
+        jnp.concatenate(ring[::-1], axis=0), (lax.axis_index("kv") + 1) * ring[0].shape[0], axis=0
+    )
     length = portion.shape[0]
     ends = jnp.arange(length, dtype=jnp.int32) * CMP_STRIDE + CMP_LEN - 1
     scores = (

time: 242 us -> 245 us (1.012)
  waiting for transfers between devices: 86.8 us -> 124 us
  blocking collectives: 35 us -> 0 us
  starting transfers between devices: 1.32 us -> 5.1 us
    ppermute x0 -> x7, waiting for transfers between devices: none -> 40.5 us  [on_device(): lax.ppermute(ring[-1], 'kv', [(dev, (dev + 1) % 8) for dev in range(8)])]
    all_gather x1 -> x0, blocking collectives: 35 us -> none  [on_device(): portion = lax.all_gather(summaries, 'kv', axis=0, tiled=True)]
    ppermute x0 -> x7, starting transfers between devices: none -> 3.77 us  [on_device(): lax.ppermute(ring[-1], 'kv', [(dev, (dev + 1) % 8) for dev in range(8)])]
    reduce_scatter x1, waiting for transfers between devices: 86.7 us -> 83.2 us  [on_device(): lax.psum_scatter(jnp.dot(blended, output_weight, preferred_element_type=j...]
  transfers between devices with their start and end apart: 3 -> 10, of which waited for: 1 -> 8; matrix products, arithmetic and copies ran while one was open for 14% -> 13% of each run, Pallas kernels for 0% -> 0%
where the time goes in v1:
time: 245 us; the launch traced here: 244 us
  waiting for transfers between devices  124 us (51%)
  matrix products  60.5 us (25%)
  other arithmetic  24.7 us (10%)
  local copies, waits for them, and re-layouts  15.3 us (6%)
  between operations  13.9 us (6%)
  starting transfers between devices  5.1 us (2%)
    reduce_scatter x1, waiting for transfers between devices, on_device(): lax.psum_scatter(jnp.dot(blended, output_weight, preferred_element_type=j...  83.2 us
    ppermute x7, waiting for transfers between devices, on_device(): lax.ppermute(ring[-1], 'kv', [(dev, (dev + 1) % 8) for dev in range(8)])  40.5 us
    dot_general x2, matrix products, online_step(): jnp.einsum('grqk,kgd->grqd', weights.astype(jnp.bfloat16), values, prefer...  18.2 us
    dot_general x1, matrix products, span_step(): jnp.einsum('qgrd,kgd->grqk', queries, stretch[..., :HD], preferred_elemen...  15.2 us
    reduce_sum x2, other arithmetic, online_step(): summed = summed * shrink + jnp.sum(weights, -1)  15.2 us
    and x1, local copies, waits for them, and re-layouts, span_step(): listed & (key_positions[None, None, :] <= positions[None, :, None])  6.03 us
  transfers between devices with their start and end apart: 10, of which 8 were waited for; matrix products, arithmetic and copies ran while one was open for 13% of the time, Pallas kernels for 0%

profile of v1, /device:TPU:0, one launch (start us, length us, event | category | flops | bytes accessed | tf_op | source)
XLA Modules:
  0.0 243.6 jit_solution(2943875160501650842)
XLA Ops:
  6.6 2.7 %convolution_convert_fusion.1 = bf16[512,128]{0,1:T(8,128)(2,1)S(1)} fusion(bf16[512,2048]{1,0:T(8,128)(2,1)} %param.17, bf16[2048,128]{1,0:T(8,128)(2,1)} %param.20), kind=kOutput, calls=%fused_computation.44 | convolution fusion | flops 268500992 | bytes 2752512 | tf_op jit(solution)/shard_map/dot_general | solution.py:94
  9.2 2.5 %fusion.91 = f32[512,128]{0,1:T(8,128)S(1)} fusion(bf16[512,2048]{1,0:T(8,128)(2,1)} %param.17, bf16[2048,128]{1,0:T(8,128)(2,1)} %param.19), kind=kOutput, calls=%fused_computation.135 | convolution fusion | flops 268435456 | bytes 2883584 | tf_op jit(solution)/shard_map/dot_general | solution.py:88
  11.7 0.3 multiply_cosine_fusion
  12.1 0.7 pad_maximum_fusion.4
  12.9 2.4 convolution_convert_fusion.2
  15.3 0.2 copy.53
  15.5 2.5 %convolution_convert_fusion.3 = bf16[512,128]{0,1:T(8,128)(2,1)S(1)} fusion(bf16[512,2048]{1,0:T(8,128)(2,1)} %param.17, bf16[2048,128]{1,0:T(8,128)(2,1)} %param.21), kind=kOutput, calls=%fused_computation.46 | convolution fusion | flops 268500992 | bytes 2752512 | tf_op jit(solution)/shard_map/dot_general | solution.py:100
  18.0 0.2 copy.52
  18.3 1.3 collective-permute-start
  19.6 4.5 %fusion.90 = f32[512,512]{0,1:T(8,128)} fusion(bf16[512,2048]{1,0:T(8,128)(2,1)} %param.17, bf16[2048,512]{1,0:T(8,128)(2,1)} %param.18), kind=kOutput, calls=%fused_computation.134 | convolution fusion | flops 1073741824 | bytes 5242880 | tf_op jit(solution)/shard_map/dot_general | solution.py:81
  25.0 0.3 copy.54
  25.2 1.0 pad_maximum_fusion
  26.2 1.0 slice_bitcast_fusion.1
  27.4 0.5 reshape.283
  27.9 1.4 convolution_convert_fusion.4
  29.5 0.5 reshape.281
  29.9 1.4 fusion.62
  31.7 3.8 %collective-permute-start.1 = (bf16[32,2,128]{0,2,1:T(8,128)(2,1)S(1)}, bf16[32,2,128]{0,2,1:T(8,128)(2,1)S(1)}, u32[]{:S(2)}, u32[]{:S(2)}) collective-permute-start(bf16[32,2,128]{0,2,1:T(8,128)(2,1)S(1)} %pad_maximum_fusion.5), channel_id=1, source_target_pairs={{0,4},{4,8},{8,12},{12,16},{16,20},{20,24},{24,28},{28,0},{1,5},{5... | collective-permute-start | bytes 49160 | tf_op jit(solution)/shard_map/ppermute | solution.py:135
  35.4 2.3 fusion.34
  37.7 3.9 %collective-permute-done.1 = bf16[32,2,128]{0,2,1:T(8,128)(2,1)S(1)} collective-permute-done((bf16[32,2,128]{0,2,1:T(8,128)(2,1)S(1)}, bf16[32,2,128]{0,2,1:T(8,128)(2,1)S(1)}, u32[]{:S(2)}, u32[]{:S(2)}) %collective-permute-start.1) | collective-permute-done | bytes 16416 | tf_op jit(solution)/shard_map/ppermute | solution.py:135
  41.6 2.9 %fusion.37 = f32[512,8]{0,1:T(8,128)} fusion(bf16[512,2048]{1,0:T(8,128)(2,1)} %param.17, bf16[2,2048,8]{1,2,0:T(8,128)(2,1)} %param.27), kind=kOutput, calls=%fused_computation.55 | convolution fusion | flops 16789504 | bytes 2146304 | tf_op jit(solution)/shard_map/dot_general | solution.py:189
  44.5 4.3 %collective-permute-done.2 = bf16[32,2,128]{0,2,1:T(8,128)(2,1)S(1)} collective-permute-done((bf16[32,2,128]{0,2,1:T(8,128)(2,1)S(1)}, bf16[32,2,128]{0,2,1:T(8,128)(2,1)S(1)}, u32[]{:S(2)}, u32[]{:S(2)}) %collective-permute-start.2) | collective-permute-done | bytes 16416 | tf_op jit(solution)/shard_map/ppermute | solution.py:135
  48.8 1.0 subtract_convert_fusion
  49.9 6.9 %collective-permute-done.3 = bf16[32,2,128]{0,2,1:T(8,128)(2,1)S(1)} collective-permute-done((bf16[32,2,128]{0,2,1:T(8,128)(2,1)S(1)}, bf16[32,2,128]{0,2,1:T(8,128)(2,1)S(1)}, u32[]{:S(2)}, u32[]{:S(2)}) %collective-permute-start.3) | collective-permute-done | bytes 16416 | tf_op jit(solution)/shard_map/ppermute | solution.py:135
  56.8 7.1 %collective-permute-done.4 = bf16[32,2,128]{0,2,1:T(8,128)(2,1)S(1)} collective-permute-done((bf16[32,2,128]{0,2,1:T(8,128)(2,1)S(1)}, bf16[32,2,128]{0,2,1:T(8,128)(2,1)S(1)}, u32[]{:S(2)}, u32[]{:S(2)}) %collective-permute-start.4) | collective-permute-done | bytes 16416 | tf_op jit(solution)/shard_map/ppermute | solution.py:135
  63.9 7.3 %collective-permute-done.5 = bf16[32,2,128]{0,2,1:T(8,128)(2,1)S(1)} collective-permute-done((bf16[32,2,128]{0,2,1:T(8,128)(2,1)S(1)}, bf16[32,2,128]{0,2,1:T(8,128)(2,1)S(1)}, u32[]{:S(2)}, u32[]{:S(2)}) %collective-permute-start.5) | collective-permute-done | bytes 16416 | tf_op jit(solution)/shard_map/ppermute | solution.py:135
  71.4 6.8 %collective-permute-done.6 = bf16[32,2,128]{0,2,1:T(8,128)(2,1)S(1)} collective-permute-done((bf16[32,2,128]{0,2,1:T(8,128)(2,1)S(1)}, bf16[32,2,128]{0,2,1:T(8,128)(2,1)S(1)}, u32[]{:S(2)}, u32[]{:S(2)}) %collective-permute-start.6) | collective-permute-done | bytes 16416 | tf_op jit(solution)/shard_map/ppermute | solution.py:135
  78.2 0.8 pad_maximum_fusion.1
  79.0 0.6 reshape.285
  79.6 1.3 reshape.278
  80.9 4.2 %collective-permute-done.7 = bf16[32,2,128]{0,2,1:T(8,128)(2,1)S(1)} collective-permute-done((bf16[32,2,128]{0,2,1:T(8,128)(2,1)S(1)}, bf16[32,2,128]{0,2,1:T(8,128)(2,1)S(1)}, u32[]{:S(2)}, u32[]{:S(2)}) %collective-permute-start.7) | collective-permute-done | bytes 16416 | tf_op jit(solution)/shard_map/ppermute | solution.py:135
  85.1 1.4 concatenate.50
  86.5 2.0 fusion.21
  88.5 2.0 copy-done.2
  90.6 0.9 fusion.24
  91.5 0.6 exponential_multiply_fusion
  92.3 55.1 %while.20 = (s32[]{:T(128)}, f32[2,4,512]{2,1,0:T(4,128)S(1)}, f32[2,4,512]{2,1,0:T(4,128)S(1)}, f32[2,4,512,64]{2,3,1,0:T(8,128)S(1)}, s32[]{:T(128)}, /*index=...) while((s32[]{:T(128)}, f32[2,4,512]{2,1,0:T(4,128)S(1)}, ...), condition=%wide.region_8.9_spmd.clone, body=%wide.region_2.8_spmd.clone.sunk | while | flops 2245501440 | bytes 127838584 | solution.py:186
  92.5 54.8 %conditional.3 = ((f32[2,4,512]{2,1,0:T(4,128)S(1)}, f32[2,4,512]{2,1,0:T(4,128)S(1)}, f32[2,4,512,64]{2,3,1,0:T(8,128)S(1)})) conditional(s32[]{:T(128)} %convert_element_type.107, (f32[2,4,512]{2,1,0:T(4,128)S(1)}, f32[2,4,512]{2,1,0:T(4,128)S(1)}, f32[2,4,512,64]{2,3,1,0:T(8,128)S(1)}) %tuple.69, (s32[2,16,16]{2,1,0:T(8,128)S(1)}, s32[]{:T(128)}, ...), branch_computations={%region_3.3_spmd, %region_4.7_spmd} | conditional | flops 2245501440 | bytes 127836296 | solution.py:176
  92.6 0.7 broadcast_compare_fusion
  93.3 1.0 compare_reduce_fusion
  94.3 2.6 %bitcast_and_fusion = pred[2,512,2048]{2,1,0:T(8,128)(4,1)} fusion(pred[512,2048]{1,0:T(8,128)(4,1)S(1)} %broadcast_compare_fusion, pred[2,16,2048]{2,1,0:T(8,128)(4,1)S(1)} %compare_reduce_fusion), kind=kLoop, calls=%fused_computation.10 | loop fusion | flops 2097152 | bytes 3211264 | tf_op jit(solution)/shard_map/while/body/eval_jaxpr/cond/branch_1_fun/and | solution.py:159
  96.9 6.0 %copy.48 = pred[2,512,2048]{1,2,0:T(8,128)(4,1)} copy(pred[2,512,2048]{2,1,0:T(8,128)(4,1)} %bitcast_and_fusion) | data formatting | bytes 4194304 | tf_op jit(solution)/shard_map/while/body/eval_jaxpr/cond/branch_1_fun/and | solution.py:159
  103.0 15.2 %fusion.2 = (f32[2,4,512]{2,1,0:T(4,128)S(1)}, f32[2,2048,512,4]{2,1,3,0:T(8,128)}) fusion(pred[2,512,2048]{1,2,0:T(8,128)(4,1)} %copy.48, bf16[512,2,4,64]{0,3,2,1:T(8,128)(2,1)} %get-tuple-element.301, bf16[4096,2,128]{0,2,1:T(8,128)(2,1)} %get-tuple-element.300, s32[]{:T(128)S(6)} %select_n.46), kind=kOutput, calls=%fused_computation.3 | convolution fusion | flops 1098903552 | bytes 36716548 | tf_op jit(solution)/shard_map/while/body/eval_jaxpr/cond/branch_1_fun/qgrd,kgd->grqk/dot_general | solution.py:161
  118.2 14.3 %fusion.6 = f32[2,4,512]{2,1,0:T(4,128)S(1)} fusion(f32[2,2048,512,4]{2,1,3,0:T(8,128)} %get-tuple-element.369, f32[2,4,512]{2,1,0:T(4,128)S(1)} %max.12, pred[2,512,2048]{1,2,0:T(8,128)(4,1)S(1)} %copy-done.1), kind=kLoop, calls=%fused_computation.7 | loop fusion | flops 33550336 | bytes 35684352 | tf_op jit(solution)/shard_map/while/body/eval_jaxpr/cond/branch_1_fun/reduce_sum | solution.py:51
  132.6 14.8 %fusion.10 = f32[2,4,512,64]{2,3,1,0:T(8,128)S(1)} fusion(f32[2,2048,512,4]{2,1,3,0:T(8,128)} %get-tuple-element.369, f32[2,4,512]{2,1,0:T(4,128)S(1)} %max.12, pred[2,512,2048]{1,2,0:T(8,128)(4,1)} %copy.48, f32[2,4,512,64]{2,3,1,0:T(8,128)S(1)} %get-tuple-element.303, bf16[4096,2,128]{0,2,1:T(8,128)(2,1)} %get-tuple-element.300, s32[]{:T(128)S(6)} %select_n.46, ...), kind=kOutput, calls=%fused_computation.13 | convolution fusion | flops 1107820544 | bytes 38305800 | tf_op jit(solution)/shard_map/while/body/eval_jaxpr/cond/branch_1_fun/grqk,kgd->grqd/dot_general | solution.py:52
  147.5 3.4 %add_convert_fusion = bf16[2,4,512,64]{2,3,1,0:T(8,128)(2,1)S(1)} fusion(f32[2,4,512,64]{2,3,1,0:T(8,128)S(1)} %get-tuple-element.319, f32[2,256,512,4]{2,1,3,0:T(8,128)} %copy-done.2, f32[2,4,512]{2,1,0:T(4,128)S(1)} %copy-done.15, pred[512,256]{0,1:T(8,128)(4,1)S(1)} %copy-done.7, f32[2,4,512]{2,1,0:T(4,128)S(1)} %get-tuple-element.320, ...), kind=kOutput, calls=%fused_computation.56 | convolution fusion | flops 140247040 | bytes 6062088 | tf_op jit(solution)/shard_map/grqk,kgd->grqd/dot_general | solution.py:52
  150.9 2.6 %convolution_convert_fusion = bf16[512,2048]{1,0:T(8,128)(2,1)} fusion(bf16[512,512]{0,1:T(8,128)(2,1)S(1)} %bitcast.140, bf16[512,2048]{1,0:T(8,128)(2,1)S(1)} %copy-done), kind=kOutput, calls=%fused_computation.40 | convolution fusion | flops 1074790400 | bytes 4718592 | tf_op jit(solution)/shard_map/dot_general | solution.py:207
  153.5 83.2 %reduce-scatter.2.cloned.1.call-done = bf16[128,2048]{1,0:T(8,128)(2,1)} async-done(((bf16[512,2048]{1,0:T(8,128)(2,1)}), bf16[128,2048]{1,0:T(8,128)(2,1)}) %reduce-scatter.2.cloned.1.call-update) | async-done | bytes 524304 | tf_op jit(solution)/shard_map/reduce_scatter | solution.py:206
  (89 shorter events, 2.1 us)
Async XLA Ops:
  6.5 144.3 %copy-start = (bf16[512,2048]{1,0:T(8,128)(2,1)S(1)}, bf16[512,2048]{1,0:T(8,128)(2,1)}, u32[]{:S(2)}) copy-start(bf16[512,2048]{1,0:T(8,128)(2,1)} %param.28) | copy-start | bytes 6291460
  6.5 6.4 %copy-start.8 = (bf16[2048,128]{1,0:T(8,128)(2,1)S(1)}, bf16[2048,128]{1,0:T(8,128)(2,1)}, u32[]{:S(2)}) copy-start(bf16[2048,128]{1,0:T(8,128)(2,1)} %param.22) | copy-start | bytes 1572868
  6.5 85.6 %all-gather.2.cloned.1.call-start = ((), (), s32[]{:S(2)}) async-start(), calls=%async_computation.1 | async-start | bytes 2359296 | tf_op jit(solution)/shard_map/all_gather | solution.py:178
  12.1 6.0 %copy-start.5 = (f32[512,32]{0,1:T(8,128)}, f32[512,32]{0,1:T(8,128)S(1)}, u32[]{:S(2)}) copy-start(f32[512,32]{0,1:T(8,128)S(1)} %get-tuple-element.385) | copy-start | bytes 196612
  12.9 223.9 %reduce-scatter.2.cloned.1.call-start = ((), (), s32[]{:S(2)}) async-start(), calls=%async_computation.2 | async-start | bytes 2621440 | tf_op jit(solution)/shard_map/reduce_scatter | solution.py:206
  18.3 6.5 %collective-permute-start = (bf16[16,2,128]{2,0,1:T(8,128)(2,1)S(1)}, bf16[16,2,128]{2,0,1:T(8,128)(2,1)S(1)}, u32[]{:S(2)}, u32[]{:S(2)}) collective-permute-start(bf16[16,2,128]{2,0,1:T(8,128)(2,1)S(1)} %pad_maximum_fusion.6), channel_id=1, source_target_pairs={{4,0},{8,4},{12,8},{16,12},{20,16},{24,20},{28,24},{5,1},{9,5},{13... | collective-permute-start | bytes 24584 | tf_op jit(solution)/shard_map/ppermute | solution.py:17
  24.1 3.8 %copy-start.16 = (bf16[128,64]{0,1:T(8,128)(2,1)S(1)}, bf16[128,64]{0,1:T(8,128)(2,1)}, u32[]{:S(2)}) copy-start(bf16[128,64]{0,1:T(8,128)(2,1)} %param.26) | copy-start | bytes 49156
  25.0 5.0 %copy-start.17 = (bf16[128,64]{0,1:T(8,128)(2,1)S(1)}, bf16[128,64]{0,1:T(8,128)(2,1)}, u32[]{:S(2)}) copy-start(bf16[128,64]{0,1:T(8,128)(2,1)} %param.24) | copy-start | bytes 49156
  31.3 17.5 %copy-start.3 = (f32[512,512]{0,1:T(8,128)S(1)}, f32[512,512]{0,1:T(8,128)}, u32[]{:S(2)}) copy-start(f32[512,512]{0,1:T(8,128)} %fusion.90) | copy-start | bytes 3145732
  31.7 10.0 %collective-permute-start.1 = (bf16[32,2,128]{0,2,1:T(8,128)(2,1)S(1)}, bf16[32,2,128]{0,2,1:T(8,128)(2,1)S(1)}, u32[]{:S(2)}, u32[]{:S(2)}) collective-permute-start(bf16[32,2,128]{0,2,1:T(8,128)(2,1)S(1)} %pad_maximum_fusion.5), channel_id=1, source_target_pairs={{0,4},{4,8},{8,12},{12,16},{16,20},{20,24},{24,28},{28,0},{1,5},{5... | collective-permute-start | bytes 49160 | tf_op jit(solution)/shard_map/ppermute | solution.py:135
  41.6 7.2 %copy-start.11 = (bf16[32,2,128]{0,2,1:T(8,128)(2,1)}, bf16[32,2,128]{0,2,1:T(8,128)(2,1)S(1)}, u32[]{:S(2)}) copy-start(bf16[32,2,128]{0,2,1:T(8,128)(2,1)S(1)} %collective-permute-done.1) | copy-start | bytes 49156
  41.6 7.2 %collective-permute-start.2 = (bf16[32,2,128]{0,2,1:T(8,128)(2,1)S(1)}, bf16[32,2,128]{0,2,1:T(8,128)(2,1)S(1)}, u32[]{:S(2)}, u32[]{:S(2)}) collective-permute-start(bf16[32,2,128]{0,2,1:T(8,128)(2,1)S(1)} %collective-permute-done.1), channel_id=1, source_target_pairs={{0,4},{4,8},{8,12},{12,16},{16,20},{20,24},{24,28},{28,0},{1,5},{5... | collective-permute-start | bytes 49160 | tf_op jit(solution)/shard_map/ppermute | solution.py:135
  48.8 22.4 %copy-start.12 = (bf16[32,2,128]{0,2,1:T(8,128)(2,1)}, bf16[32,2,128]{0,2,1:T(8,128)(2,1)S(1)}, u32[]{:S(2)}) copy-start(bf16[32,2,128]{0,2,1:T(8,128)(2,1)S(1)} %collective-permute-done.2) | copy-start | bytes 49156
  48.8 8.0 %collective-permute-start.3 = (bf16[32,2,128]{0,2,1:T(8,128)(2,1)S(1)}, bf16[32,2,128]{0,2,1:T(8,128)(2,1)S(1)}, u32[]{:S(2)}, u32[]{:S(2)}) collective-permute-start(bf16[32,2,128]{0,2,1:T(8,128)(2,1)S(1)} %collective-permute-done.2), channel_id=1, source_target_pairs={{0,4},{4,8},{8,12},{12,16},{16,20},{20,24},{24,28},{28,0},{1,5},{5... | collective-permute-start | bytes 49160 | tf_op jit(solution)/shard_map/ppermute | solution.py:135
  49.8 28.3 %copy-start.4 = (bf16[512,8,32]{0,2,1:T(8,128)(2,1)}, bf16[512,8,32]{0,2,1:T(8,128)(2,1)S(1)}, u32[]{:S(2)}) copy-start(bf16[512,8,32]{0,2,1:T(8,128)(2,1)S(1)} %get-tuple-element.373) | copy-start | bytes 786436
  56.8 14.4 %copy-start.13 = (bf16[32,2,128]{0,2,1:T(8,128)(2,1)}, bf16[32,2,128]{0,2,1:T(8,128)(2,1)S(1)}, u32[]{:S(2)}) copy-start(bf16[32,2,128]{0,2,1:T(8,128)(2,1)S(1)} %collective-permute-done.3) | copy-start | bytes 49156
  56.8 7.1 %collective-permute-start.4 = (bf16[32,2,128]{0,2,1:T(8,128)(2,1)S(1)}, bf16[32,2,128]{0,2,1:T(8,128)(2,1)S(1)}, u32[]{:S(2)}, u32[]{:S(2)}) collective-permute-start(bf16[32,2,128]{0,2,1:T(8,128)(2,1)S(1)} %collective-permute-done.3), channel_id=1, source_target_pairs={{0,4},{4,8},{8,12},{12,16},{16,20},{20,24},{24,28},{28,0},{1,5},{5... | collective-permute-start | bytes 49160 | tf_op jit(solution)/shard_map/ppermute | solution.py:135
  63.9 7.3 %collective-permute-start.5 = (bf16[32,2,128]{0,2,1:T(8,128)(2,1)S(1)}, bf16[32,2,128]{0,2,1:T(8,128)(2,1)S(1)}, u32[]{:S(2)}, u32[]{:S(2)}) collective-permute-start(bf16[32,2,128]{0,2,1:T(8,128)(2,1)S(1)} %collective-permute-done.4), channel_id=1, source_target_pairs={{0,4},{4,8},{8,12},{12,16},{16,20},{20,24},{24,28},{28,0},{1,5},{5... | collective-permute-start | bytes 49160 | tf_op jit(solution)/shard_map/ppermute | solution.py:135
  71.2 7.0 %collective-permute-start.6 = (bf16[32,2,128]{0,2,1:T(8,128)(2,1)S(1)}, bf16[32,2,128]{0,2,1:T(8,128)(2,1)S(1)}, u32[]{:S(2)}, u32[]{:S(2)}) collective-permute-start(bf16[32,2,128]{0,2,1:T(8,128)(2,1)S(1)} %collective-permute-done.5), channel_id=1, source_target_pairs={{0,4},{4,8},{8,12},{12,16},{16,20},{20,24},{24,28},{28,0},{1,5},{5... | collective-permute-start | bytes 49160 | tf_op jit(solution)/shard_map/ppermute | solution.py:135
  71.3 20.1 %copy-start.6 = (pred[512,256]{0,1:T(8,128)(4,1)}, pred[512,256]{0,1:T(8,128)(4,1)S(1)}, u32[]{:S(2)}) copy-start(pred[512,256]{0,1:T(8,128)(4,1)S(1)} %broadcast_compare_fusion.1) | copy-start | bytes 393220
  78.2 7.0 %collective-permute-start.7 = (bf16[32,2,128]{0,2,1:T(8,128)(2,1)S(1)}, bf16[32,2,128]{0,2,1:T(8,128)(2,1)S(1)}, u32[]{:S(2)}, u32[]{:S(2)}) collective-permute-start(bf16[32,2,128]{0,2,1:T(8,128)(2,1)S(1)} %collective-permute-done.6), channel_id=1, source_target_pairs={{0,4},{4,8},{8,12},{12,16},{16,20},{20,24},{24,28},{28,0},{1,5},{5... | collective-permute-start | bytes 49160 | tf_op jit(solution)/shard_map/ppermute | solution.py:135
  86.5 5.0 %copy-start.10 = (bf16[512,2,128]{0,2,1:T(8,128)(2,1)}, bf16[512,2,128]{0,2,1:T(8,128)(2,1)S(1)}, u32[]{:S(2)}) copy-start(bf16[512,2,128]{0,2,1:T(8,128)(2,1)S(1)} %concatenate.50) | copy-start | bytes 786436
  86.5 5.7 %copy-start.9 = (s32[2,16,16]{2,1,0:T(8,128)S(1)}, s32[2,16,16]{2,1,0:T(8,128)}, u32[]{:S(2)}) copy-start(s32[2,16,16]{2,1,0:T(8,128)} %param.29) | copy-start | bytes 6148
  88.5 2.1 copy-start.2
  88.5 3.6 %copy-start.14 = (f32[2,4,512]{2,1,0:T(4,128)}, f32[2,4,512]{2,1,0:T(4,128)S(1)}, u32[]{:S(2)}) copy-start(f32[2,4,512]{2,1,0:T(4,128)S(1)} %broadcast_maximum_fusion) | copy-start | bytes 49156
  92.3 55.2 %copy-start.7 = (pred[512,256]{0,1:T(8,128)(4,1)S(1)}, pred[512,256]{0,1:T(8,128)(4,1)}, u32[]{:S(2)}) copy-start(pred[512,256]{0,1:T(8,128)(4,1)} %copy-done.6) | copy-start | bytes 393220
  92.3 55.2 %copy-start.15 = (f32[2,4,512]{2,1,0:T(4,128)S(1)}, f32[2,4,512]{2,1,0:T(4,128)}, u32[]{:S(2)}) copy-start(f32[2,4,512]{2,1,0:T(4,128)} %copy-done.14) | copy-start | bytes 49156
  92.3 55.2 %copy-start.18 = (f32[512,2,4]{0,2,1:T(4,128)S(1)}, f32[512,2,4]{0,2,1:T(4,128)}, u32[]{:S(2)}) copy-start(f32[512,2,4]{0,2,1:T(4,128)} %reshape.285) | copy-start | bytes 49156
  92.3 55.2 %copy-start.19 = (f32[512,2,4]{0,2,1:T(4,128)S(1)}, f32[512,2,4]{0,2,1:T(4,128)}, u32[]{:S(2)}) copy-start(f32[512,2,4]{0,2,1:T(4,128)} %reshape.278) | copy-start | bytes 49156
  92.3 55.2 %copy-start.20 = (f32[2,4,512]{2,1,0:T(4,128)S(1)}, f32[2,4,512]{2,1,0:T(4,128)}, u32[]{:S(2)}) copy-start(f32[2,4,512]{2,1,0:T(4,128)} %get-tuple-element.382) | copy-start | bytes 49156
  92.3 55.2 %copy-start.21 = (f32[2,4,512]{2,1,0:T(4,128)S(1)}, f32[2,4,512]{2,1,0:T(4,128)}, u32[]{:S(2)}) copy-start(f32[2,4,512]{2,1,0:T(4,128)} %get-tuple-element.383) | copy-start | bytes 49156
  103.0 15.2 %copy-start.1 = (pred[2,512,2048]{1,2,0:T(8,128)(4,1)S(1)}, pred[2,512,2048]{1,2,0:T(8,128)(4,1)}, u32[]{:S(2)}) copy-start(pred[2,512,2048]{1,2,0:T(8,128)(4,1)} %copy.48) | copy-start | bytes 6291460 | tf_op jit(solution)/shard_map/while/body/eval_jaxpr/cond
Sparse Core Ops, SparseCore 0:
  13.0 56.1 all-gather.1
  153.6 83.0 reduce-scatter.1
